TPU v7x, 256 devices: a whole 4x4x8 slice. The times are simulated.
256 devices in a mesh: ep: 32 (over z, x), tp: 8 (over y, core).
Axes of the slice: x: 4, y: 4, z: 8, core: 2. Of those that a mesh axis runs over, the one named last changes fastest.
Arguments:
- queries: bfloat16 [32768, 2048], P('ep', 'tp'), may hold values from -6 to 6
- key_vectors: bfloat16 [32768, 2048], P('ep', 'tp'), may hold values from -6 to 6
- value_vectors: bfloat16 [32768, 4096], P('ep', 'tp'), may hold values from -6 to 6
- decay_logit: float32 [32768, 2048], P('ep', 'tp'), may hold values from -11 to 16
- head_gain: float32 [256], replicated, may hold values from 0.1 to 1.9
- routed_rows: bfloat16 [8192, 4096], P('ep'), may hold values from -6 to 6
- pre_gain: float32 [4096], replicated, may hold values from 0.1 to 1.9
- expert_pick: int32 [8192, 2], P('ep'), may hold values from 0 to 31, as said below
- route_weight: float32 [8192, 2], P('ep'), may hold values from 0.2 to 1
- gate_weight: bfloat16 [32, 4096, 2048], P('ep', None, 'tp'), may hold values from -0.09375 to 0.09375
- up_weight: bfloat16 [32, 4096, 2048], P('ep', None, 'tp'), may hold values from -0.09375 to 0.09375
- down_weight: bfloat16 [32, 2048, 4096], P('ep', 'tp'), may hold values from -0.125 to 0.125
- post_gain: float32 [4096], replicated, may hold values from 0.1 to 1.9
Outputs:
- mixed_heads: bfloat16 [32768, 4096], P('ep', 'tp')
- routed_out: bfloat16 [8192, 4096], P(('ep', 'tp'))
Inputs may be any that keep to these rules, and one draw needn't show every extreme that they name: `expert_pick`: each row names 2 different experts, both in the same one of 4 equal groups of consecutive expert numbers. In every aligned block of 32 rows no expert is named more than 4 times, and some expert exactly 4 times.
All inputs are finite; a program needn't handle non-finite values.
Results may differ from a plain program's by a relative error of at most 0.015.
Values may be sent and summed in bfloat16 or wider, within the bound.
A program may use at most 128 MiB of HBM per device.

v0:
```python
import jax
import jax.numpy as jnp
from jax import lax
from jax.sharding import Mesh
from jax.sharding import PartitionSpec as P

DK = 128
DV = 256
BLK = 64
EP = ("ep_0", "ep_1")
EP_TP = ("ep_0", "ep_1", "tp")


def neutral_like(x, identity):
    return jax.tree.map(
        lambda part, zero: jnp.zeros_like(part) + jnp.asarray(zero, part.dtype), x, identity
    )


def prefix_by_axis(x, axes, combine, identity):
    before = start = neutral_like(x, identity)
    running = x
    for axis in reversed(axes):
        length, index = (lax.axis_size(axis), lax.axis_index(axis))
        pieces = jax.tree.map(
            lambda part, kind: lax.all_gather(part.astype(kind), axis),
            running,
            (jnp.bfloat16, jnp.bfloat16),
        )
        inside, running = (start, start)
        for k in range(length):
            passed = k < index
            running = combine(
                running, jax.tree.map(lambda part, own: part[k].astype(own.dtype), pieces, x)
            )
            inside = jax.tree.map(lambda new, old: jnp.where(passed, new, old), running, inside)
        before = combine(inside, before)
    return before


def chain_join(earlier, later_part):
    decay_first, initial_memory_matrix = earlier
    decay_second, state_second = later_part
    return (
        decay_first * decay_second,
        initial_memory_matrix * decay_second[..., None] + state_second,
    )


def row_norm(values, gain):
    return values * lax.rsqrt(jnp.mean(values * values, axis=-1, keepdims=True) + 1e-06) * gain


def token_mixer(queries, key_vectors, value_vectors, decay_logit, head_gain):
    blocks = queries.shape[0] // BLK
    heads_here = queries.shape[1] // DK
    key_shape = (blocks, BLK, heads_here, DK)
    log_rate = jax.nn.log_sigmoid(decay_logit).reshape(key_shape) / 16.0
    cumulative = jnp.cumsum(log_rate, axis=1)
    ending = cumulative[:, -1]
    query_rows = queries.reshape(key_shape)
    key_rows = key_vectors.reshape(key_shape)
    value_rows = value_vectors.reshape(blocks, BLK, heads_here, DV)
    query_decay = (query_rows * jnp.exp(cumulative)).astype(jnp.bfloat16)
    key_decay = (key_rows * jnp.exp(-cumulative)).astype(jnp.bfloat16)
    key_to_end = (key_rows * jnp.exp(ending[:, None] - cumulative)).astype(jnp.bfloat16)
    update = jnp.einsum(
        "njhd,njhe->nhde", key_to_end, value_rows, preferred_element_type=jnp.float32
    )
    step_decay = jnp.exp(ending)

    def advance(carry, inputs):
        carry_state, carry_decay = carry
        block_update, block_decay = inputs
        next_carry = (
            carry_state * block_decay[..., None] + block_update,
            carry_decay * block_decay,
        )
        return (next_carry, (carry_state, carry_decay))

    start_carry = (jnp.zeros_like(update[0]), jnp.ones_like(step_decay[0]))
    (final_state, total_decay), (local_states, local_decay) = lax.scan(
        advance, start_carry, (update, step_decay)
    )
    incoming = prefix_by_axis(
        (total_decay, final_state),
        EP,
        chain_join,
        (jnp.ones_like(total_decay), jnp.zeros_like(final_state)),
    )
    causal_mask = jnp.tril(jnp.ones((BLK, BLK), dtype=bool))
    scores = jnp.einsum(
        "nihd,njhd->nhij", query_decay, key_decay, preferred_element_type=jnp.float32
    )
    weights = jnp.where(causal_mask, scores, 0.0).astype(jnp.bfloat16)
    inside = jnp.einsum("nhij,njhe->nihe", weights, value_rows, preferred_element_type=jnp.float32)
    states = (local_states + incoming[1][None] * local_decay[..., None]).astype(jnp.bfloat16)
    carried = jnp.einsum("nihd,nhde->nihe", query_decay, states, preferred_element_type=jnp.float32)
    outputs = row_norm(inside + carried, head_gain).astype(jnp.bfloat16)
    return outputs.reshape(queries.shape[0], heads_here * DV)


def routed_experts(
    routed_rows, pre_gain, expert_pick, route_weight, gate_weight, up_weight, down_weight, post_gain
):
    tp_count = lax.axis_size("tp")
    ep_count = lax.axis_size(EP)
    part_index = lax.axis_index("tp")
    ep_rows, model_width = routed_rows.shape
    part_rows = ep_rows // tp_count
    top_count = expert_pick.shape[1]
    experts = ep_count * gate_weight.shape[0]
    capacity = 2 * top_count * part_rows // experts
    normed = row_norm(routed_rows.astype(jnp.float32), pre_gain).astype(jnp.bfloat16)
    padded = jnp.concatenate([normed, jnp.zeros((1, model_width), jnp.bfloat16)], axis=0)
    picks = expert_pick.reshape(tp_count, part_rows * top_count)
    matches = (picks[:, :, None] == jnp.arange(experts, dtype=jnp.int32)[None, None, :]).astype(
        jnp.int32
    )
    slots = jnp.sum((jnp.cumsum(matches, axis=1) - 1) * matches, axis=2)
    targets = picks * capacity + slots
    sources = (
        jnp.arange(part_rows * top_count, dtype=jnp.int32)[None, :] // top_count
        + part_rows * jnp.arange(tp_count, dtype=jnp.int32)[:, None]
    )
    slice_offset_index = jnp.broadcast_to(
        jnp.arange(tp_count, dtype=jnp.int32)[:, None], targets.shape
    )
    table = (
        jnp.full((tp_count, experts * capacity), ep_rows, jnp.int32)
        .at[slice_offset_index, targets]
        .set(sources)
    )
    gate_local = gate_weight[0]
    up_local = up_weight[0]
    down_local = down_weight[0]
    own_table = lax.dynamic_slice_in_dim(table, part_index, 1, 0)
    outgoing = padded[own_table].reshape(1, ep_count, capacity, model_width)
    arrived = lax.all_gather(
        lax.all_to_all(outgoing, EP, split_axis=1, concat_axis=1, tiled=True),
        "tp",
        axis=0,
        tiled=True,
    )
    gate_act = jnp.einsum("pskd,df->pskf", arrived, gate_local, preferred_element_type=jnp.float32)
    up_act = jnp.einsum("pskd,df->pskf", arrived, up_local, preferred_element_type=jnp.float32)
    hidden = (jax.nn.silu(gate_act) * up_act).astype(jnp.bfloat16)
    summed = lax.psum_scatter(
        jnp.einsum("pskf,fd->pskd", hidden, down_local, preferred_element_type=jnp.float32).astype(
            jnp.bfloat16
        ),
        "tp",
        scatter_dimension=0,
        tiled=True,
    )
    returned = lax.all_to_all(summed, EP, split_axis=1, concat_axis=1, tiled=True)
    flattened = returned.reshape(experts * capacity, model_width)
    my_slots = lax.dynamic_slice_in_dim(targets, part_index, 1, 0).reshape(part_rows, top_count)
    my_weight = lax.dynamic_slice_in_dim(route_weight, part_index * part_rows, part_rows, 0)
    combined = jnp.sum(flattened[my_slots].astype(jnp.float32) * my_weight[:, :, None], axis=1)
    return row_norm(combined, post_gain).astype(jnp.bfloat16)


def on_device(
    queries,
    key_vectors,
    value_vectors,
    decay_logit,
    head_gain,
    routed_rows,
    pre_gain,
    expert_pick,
    route_weight,
    gate_weight,
    up_weight,
    down_weight,
    post_gain,
):
    mixed_heads = token_mixer(queries, key_vectors, value_vectors, decay_logit, head_gain)
    routed_out = routed_experts(
        routed_rows,
        pre_gain,
        expert_pick,
        route_weight,
        gate_weight,
        up_weight,
        down_weight,
        post_gain,
    )
    return (mixed_heads, routed_out)


def solution(mesh):
    torus = Mesh(mesh.devices.reshape(8, 4, mesh.shape["tp"]), ("ep_0", "ep_1", "tp"))
    placed = (
        P(EP, "tp"),
        P(EP, "tp"),
        P(EP, "tp"),
        P(EP, "tp"),
        P(),
        P(EP, None),
        P(),
        P(EP, None),
        P(EP, None),
        P(EP, None, "tp"),
        P(EP, None, "tp"),
        P(EP, "tp", None),
        P(),
    )
    return jax.shard_map(
        on_device,
        mesh=torus,
        in_specs=placed,
        out_specs=(P(EP, "tp"), P(EP_TP, None)),
        check_vma=False,
    )
```

profile of v0, /device:TPU:1, one launch (start us, length us, event | category | flops | bytes accessed | tf_op | source)
XLA Modules:
  0.0 287.7 jit_solution(14638093598080471657)
XLA Ops:
  11.9 22.1 %scatter_fusion = s32[8,128]{1,0:T(8,128)S(1)} fusion(s32[8,128]{1,0:T(8,128)S(1)} %broadcast_in_dim.33, s32[512]{0:T(512)S(1)} %reshape.309, s32[512]{0:T(512)S(1)} %reshape.311), kind=kCustom, calls=%fused_computation.2 | custom fusion | bytes 10240 | tf_op jit(solution)/shard_map/scatter | solution.py:132
  34.0 2.1 fusion.1
  36.1 2.2 fusion.3
  38.4 1.5 concatenate.6
  39.9 4.1 %gather_fusion = bf16[128,4096]{1,0:T(8,128)(2,1)S(1)} fusion(bf16[257,4096]{1,0:T(8,128)(2,1)} %concatenate.6, s32[1024]{0:T(1024)S(1)} %pad_clamp_fusion.1), kind=kCustom, calls=%fused_computation | custom fusion | bytes 2097664 | tf_op jit(solution)/shard_map/gather | solution.py:138
  45.2 38.0 %all_to_all.10 = bf16[1,32,4,4096]{3,2,0,1:T(4,128)(2,1)S(1)} all-to-all(bf16[1,32,4,4096]{3,2,0,1:T(4,128)(2,1)} %bitcast.178), channel_id=1, replica_groups=mesh['ep_0'=8,'ep_1'=4,'tp'=8] {'ep_0','ep_1'}, dimensions={1} | all-to-all | bytes 2097152 | tf_op jit(solution)/shard_map/all_to_all | solution.py:140
  83.3 1.6 copy.100
  85.1 1.8 fusion.20
  87.0 1.5 div.38
  88.5 2.5 reshape.280
  91.0 2.6 reshape.281
  95.0 1.4 fusion.22
  96.4 4.3 %multiply_convert_fusion.2 = (bf16[16,64,2,128]{3,0,1,2:T(8,128)(2,1)}, bf16[16,64,2,128]{3,0,1,2:T(8,128)(2,1)S(1)}, bf16[16,64,2,128]{3,0,1,2:T(8,128)(2,1)}) fusion(f32[16,64,2,128]{3,0,1,2:T(8,128)S(1)} %fusion.22, f32[16,64,2,128]{3,2,1,0:T(2,128)} %reshape.281, f32[16,2,128]{2,0,1:T(8,128)S(1)} %slice_bitcast_fusion.4, f32[16,64,2,128]{3,2,1,0:T(2,128)} %reshape.280), kind=kLoop, calls=%fused_computation.40 | loop fusion | flops 2097152 | bytes 4734976 | tf_op jit(solution)/shard_map/convert_element_type | solution.py:65
  100.7 2.7 fusion.24
  103.5 33.6 %all-gather.8.cloned.1.call-done = bf16[8,32,4,4096]{3,1,2,0:T(8,128)(2,1)} async-done(((bf16[1,32,4,4096]{3,1,2,0:T(8,128)(2,1)}), bf16[8,32,4,4096]{3,1,2,0:T(8,128)(2,1)}) %all-gather.8.cloned.1.call-update) | async-done | bytes 8388624 | tf_op jit(solution)/shard_map/all_gather | solution.py:139
  137.0 6.5 %fusion.8 = f32[8,32,4,256]{3,1,2,0:T(8,128)S(1)} fusion(bf16[8,32,4,4096]{3,1,2,0:T(8,128)(2,1)} %all-gather.8.cloned.1.call-done, bf16[1,4096,256]{2,1,0:T(8,128)(2,1)} %param.24), kind=kOutput, calls=%fused_computation.21 | convolution fusion | flops 2147483648 | bytes 11534336 | tf_op jit(solution)/shard_map/pskd,df->pskf/dot_general | solution.py:145
  144.0 2.4 fusion.15
  146.4 5.6 %convolution_convert_fusion = bf16[8,32,4,4096]{3,1,2,0:T(8,128)(2,1)} fusion(bf16[8,32,4,256]{3,1,2,0:T(8,128)(2,1)S(1)} %fusion.15, bf16[1,256,4096]{2,1,0:T(8,128)(2,1)S(1)} %copy-done), kind=kOutput, calls=%fused_computation.9 | convolution fusion | flops 2151677952 | bytes 11010048 | tf_op jit(solution)/shard_map/pskf,fd->pskd/dot_general | solution.py:149
  152.0 29.7 %while.17 = (s32[]{:T(128)}, f32[2,128,256]{2,1,0:T(8,128)S(1)}, f32[2,128]{1,0:T(2,128)S(1)}, f32[16,2,128,256]{3,2,1,0:T(8,128)}, f32[16,2,128]{2,1,0:T(2,128)...) while((s32[]{:T(128)}, f32[2,128,256]{2,1,0:T(8,128)S(1)}, ...), condition=%wide.region_2.3_spmd.clone, body=%wide.region_1.2_spmd.clone.sunk | while | flops 262915 | bytes 1319542 | solution.py:82
  181.8 8.4 %all-gather.2 = bf16[4,2,128]{2,1,0:T(2,128)(2,1)S(1)} all-gather(bf16[1,2,128]{2,1,0:T(2,128)(2,1)S(1)} %convert_bitcast_fusion.1), channel_id=2, replica_groups=mesh['ep_0'=8,'ep_1'=4,'tp'=8] {'ep_1'}, dimensions={0}, use_global_device_ids=true | all-gather | bytes 2560 | tf_op jit(solution)/shard_map/all_gather | solution.py:26
  190.3 11.3 %all-gather.1 = bf16[8,128,256]{2,1,0:T(8,128)(2,1)S(1)} all-gather(bf16[2,128,256]{2,1,0:T(8,128)(2,1)S(1)} %convert_element_type.277), channel_id=3, replica_groups=mesh['ep_0'=8,'ep_1'=4,'tp'=8] {'ep_1'}, dimensions={0}, use_global_device_ids=true | all-gather | bytes 655360 | tf_op jit(solution)/shard_map/all_gather | solution.py:26
  203.6 2.8 reduce-scatter.2.cloned.1.call-done
  206.4 3.0 %copy.101 = bf16[1,32,4,4096]{3,2,0,1:T(4,128)(2,1)} copy(bf16[1,32,4,4096]{3,1,2,0:T(8,128)(2,1)} %reduce-scatter.2.cloned.1.call-done) | data formatting | bytes 2097152 | tf_op jit(solution)/shard_map/reduce_scatter | solution.py:148
  209.4 9.7 %all-to-all-start.1 = ((bf16[1,32,4,4096]{3,2,0,1:T(4,128)(2,1)}), bf16[1,32,4,4096]{3,2,0,1:T(4,128)(2,1)}, u32[]{:S(2)}, u32[]{:S(2)}) async-start(bf16[1,32,4,4096]{3,2,0,1:T(4,128)(2,1)} %copy.101), calls=%async_computation.2 | async-start | bytes 2097152 | tf_op jit(solution)/shard_map/all_to_all | solution.py:156
  219.3 38.9 %all_gather.25 = bf16[8,2,128]{2,1,0:T(2,128)(2,1)S(1)} all-gather(bf16[1,2,128]{2,1,0:T(2,128)(2,1)S(1)} %get-tuple-element.129), channel_id=1, replica_groups=mesh['ep_0'=8,'ep_1'=4,'tp'=8] {'ep_0'}, dimensions={0}, use_global_device_ids=true | all-gather | bytes 4608 | tf_op jit(solution)/shard_map/all_gather | solution.py:26
  258.2 2.0 fusion.42
  260.2 4.7 %fusion.4 = f32[16,2,256,64]{2,3,1,0:T(8,128)} fusion(f32[16,2,128,256]{3,2,1,0:T(8,128)} %get-tuple-element.42, f32[16,2,128]{2,1,0:T(2,128)S(1)} %get-tuple-element.45, f32[2,128,256]{2,1,0:T(8,128)S(1)} %fusion.42, bf16[16,64,2,128]{3,0,1,2:T(8,128)(2,1)} %get-tuple-element.121), kind=kOutput, calls=%fused_computation.17 | convolution fusion | flops 137363456 | bytes 7094272 | tf_op jit(solution)/shard_map/nihd,nhde->nihe/dot_general | solution.py:98
  264.9 4.0 %multiply_reduce_fusion = (f32[16,64,2]{1,2,0:T(2,128)S(1)}, f32[16,64,2,256]{3,1,2,0:T(8,128)}) fusion(f32[16,2,256,64]{2,3,1,0:T(8,128)} %fusion.4, bf16[16,64,2,256]{3,2,1,0:T(2,128)(2,1)S(1)} %reshape.275, bf16[16,64,2,128]{3,0,1,2:T(8,128)(2,1)} %get-tuple-element.119, pred[64,64]{1,0:T(8,128)(4,1)S(1)} %iota_compare_fusion.3, ...), kind=kOutput, calls=%fused_computation.25 | convolution fusion | flops 102496256 | bytes 6303744 | tf_op jit(solution)/shard_map/nhij,njhe->nihe/dot_general | solution.py:96
  268.9 1.9 multiply_convert_fusion
  274.5 1.7 gather_fusion.1
  276.2 1.7 reshape.336
  277.9 1.4 multiply_reduce_fusion.1
  (155 shorter events, 43.3 us)
Async XLA Ops:
  8.0 138.4 %copy-start = (bf16[1,256,4096]{2,1,0:T(8,128)(2,1)S(1)}, bf16[1,256,4096]{2,1,0:T(8,128)(2,1)}, u32[]{:S(2)}) copy-start(bf16[1,256,4096]{2,1,0:T(8,128)(2,1)} %param.26) | copy-start | bytes 6291460
  8.0 129.0 %all-gather.8.cloned.1.call-start = ((), (), s32[]{:S(2)}) async-start(), calls=%async_computation.4 | async-start | bytes 9437184 | tf_op jit(solution)/shard_map/all_gather | solution.py:139
  11.9 24.2 %copy-start.2 = (f32[4096]{0:T(1024)S(1)}, f32[4096]{0:T(1024)}, u32[]{:S(2)}) copy-start(f32[4096]{0:T(1024)} %param.21) | copy-start | bytes 49156
  84.9 121.5 %reduce-scatter.2.cloned.1.call-start = ((), (), s32[]{:S(2)}) async-start(), calls=%async_computation.5 | async-start | bytes 9437184 | tf_op jit(solution)/shard_map/reduce_scatter | solution.py:148
  137.0 6.5 %copy-start.6 = (bf16[8,32,4,4096]{3,1,2,0:T(8,128)(2,1)S(1)}, bf16[8,32,4,4096]{3,1,2,0:T(8,128)(2,1)}, u32[]{:S(2)}) copy-start(bf16[8,32,4,4096]{3,1,2,0:T(8,128)(2,1)} %all-gather.8.cloned.1.call-done) | copy-start | bytes 25165828
  137.0 7.0 %copy-start.7 = (bf16[1,4096,256]{2,1,0:T(8,128)(2,1)S(1)}, bf16[1,4096,256]{2,1,0:T(8,128)(2,1)}, u32[]{:S(2)}) copy-start(bf16[1,4096,256]{2,1,0:T(8,128)(2,1)} %param.25) | copy-start | bytes 6291460
  152.0 106.2 %all-gather.6.cloned.1.call-start = ((), (), s32[]{:S(2)}) async-start(), calls=%async_computation.3 | async-start | bytes 1179648 | tf_op jit(solution)/shard_map/all_gather | solution.py:26
  181.8 37.3 %copy-start.5 = (f32[256,2]{0,1:T(2,128)S(1)}, f32[256,2]{0,1:T(2,128)}, u32[]{:S(2)}) copy-start(f32[256,2]{0,1:T(2,128)} %param.23) | copy-start | bytes 6148
  201.6 0.8 copy-start.1
  209.4 63.8 %all-to-all-start.1 = ((bf16[1,32,4,4096]{3,2,0,1:T(4,128)(2,1)}), bf16[1,32,4,4096]{3,2,0,1:T(4,128)(2,1)}, u32[]{:S(2)}, u32[]{:S(2)}) async-start(bf16[1,32,4,4096]{3,2,0,1:T(4,128)(2,1)} %copy.101), calls=%async_computation.2 | async-start | bytes 2097152 | tf_op jit(solution)/shard_map/all_to_all | solution.py:156
  264.9 4.0 %copy-start.4 = (f32[256]{0:T(256)S(1)}, f32[256]{0:T(256)}, u32[]{:S(2)}) copy-start(f32[256]{0:T(256)} %param.19) | copy-start | bytes 3076
  274.5 5.0 %copy-start.3 = (f32[4096]{0:T(1024)S(1)}, f32[4096]{0:T(1024)}, u32[]{:S(2)}) copy-start(f32[4096]{0:T(1024)} %param.27) | copy-start | bytes 49156
Sparse Core Ops, SparseCore 0:
  85.0 52.0 all-gather.7
  152.1 54.2 reduce-scatter.1
Sparse Core Ops, SparseCore 1:
  203.3 45.7 all-gather.5
where the time goes:
time: 292 us; the launch traced here: 288 us
  blocking collectives  96.7 us (33%)
  local copies, waits for them, and re-layouts  52.1 us (18%)
  other arithmetic  50.4 us (17%)
  waiting for transfers between devices  36.4 us (12%)
  matrix products  25.8 us (9%)
  between operations  15.9 us (5%)
  starting transfers between devices  9.97 us (3%)
    all_gather x3, blocking collectives, prefix_by_axis(): lax.all_gather(part.astype(kind), axis)  58.7 us
    all_to_all x1, blocking collectives, routed_experts(): lax.all_to_all(outgoing, EP, split_axis=1, concat_axis=1, tiled=True)  38 us
    all_gather x1, waiting for transfers between devices, routed_experts(): lax.all_gather(lax.all_to_all(outgoing, EP, split_axis=1, concat_axis=1,...  33.6 us
    scatter x1, local copies, waits for them, and re-layouts, routed_experts(): table = jnp.full((tp_count, experts * capacity), ep_rows, jnp.int32).at[s...  22.1 us
    add x16, other arithmetic, advance(): carry_state * block_decay[..., None] + block_update  17.1 us
    dynamic_update_slice x32, other arithmetic, token_mixer(): lax.scan(advance, start_carry, (update, step_decay))  11.8 us
    all_to_all x1, starting transfers between devices, routed_experts(): lax.all_to_all(summed, EP, split_axis=1, concat_axis=1, tiled=True)  9.67 us
    dot_general x1, matrix products, routed_experts(): jnp.einsum('pskd,df->pskf', arrived, gate_local, preferred_element_type=j...  6.46 us
  transfers between devices with their start and end apart: 4, of which 2 were waited for; matrix products, arithmetic and copies ran while one was open for 23% of the time, Pallas kernels for 0%

commit v1 on v0

v1 whole, which is shorter than its diff:
```python
import jax
import jax.numpy as jnp
from jax import lax
from jax.experimental import pallas as pl
from jax.experimental.pallas import tpu as pltpu
from jax.sharding import Mesh
from jax.sharding import PartitionSpec as P

BLK, DK, DV = 64, 128, 256
NZ, NX, NY = 8, 4, 4
D = 4096
MESH = pl.DeviceIdType.MESH
EP, TP = ("z", "x"), ("y", "c")
F32, BF16 = jnp.float32, jnp.bfloat16
VLIM = 60 * 1024 * 1024
NT = (((1,), (1,)), ((), ()))
TN = (((0,), (0,)), ((), ()))


def where_am_i():
    return tuple(lax.axis_index(a) for a in ("z", "x", "y", "c"))


def near(z, j):
    off = jnp.where(lax.rem(j, 2) == 1, (j + 1) // 2, NZ - j // 2)
    return lax.rem(z + off, NZ)


def remote(src, dst, ssem, rsem, **to):
    return pltpu.make_async_remote_copy(
        src_ref=src, dst_ref=dst, send_sem=ssem, recv_sem=rsem, device_id=to, device_id_type=MESH
    )


def await_bytes(ref, sem):
    pltpu.make_async_copy(ref, ref, sem).wait()


def greet(groups):
    barrier = pltpu.get_barrier_semaphore()
    total = 0
    for to, is_other in groups:
        if is_other is True:
            pl.semaphore_signal(barrier, inc=1, device_id=to, device_id_type=MESH)
            total = total + 1
        else:

            @pl.when(is_other)
            def _(to=to):
                pl.semaphore_signal(barrier, inc=1, device_id=to, device_id_type=MESH)

            total = total + is_other.astype(jnp.int32)
    pl.semaphore_wait(barrier, total)


def exchange_peers(z, x, y, c):
    peers = []
    for dz in range(NZ):
        for xh in range(2):
            zd, xd = lax.rem(z + dz, NZ), 2 * xh + c
            to = {"z": zd, "x": xd, "y": y, "c": lax.rem(x, 2)}
            peers.append((to, True if dz else jnp.logical_not((xd == x) & (lax.rem(x, 2) == c))))
    return peers


def tp_peers(y, c):
    return [
        ({"y": lax.rem(y + 1, NY)}, True),
        ({"y": lax.rem(y + NY - 1, NY)}, True),
        ({"c": 1 - c}, True),
    ]


def slot_matrix(picks, c):
    shape = (2 * 32, 128)
    r = lax.broadcasted_iota(jnp.int32, shape, 0)
    i = lax.broadcasted_iota(jnp.int32, shape, 1)
    expert = 2 * (i >> 3) + c
    same_block = (r >> 5) == ((i >> 2) & 1)
    first = (picks[:, 0:1] == expert) & same_block
    second = (picks[:, 1:2] == expert) & same_block
    named = jnp.where(first | second, 1.0, 0.0).astype(BF16)
    rr = lax.broadcasted_iota(jnp.int32, (64, 64), 0)
    cc = lax.broadcasted_iota(jnp.int32, (64, 64), 1)
    earlier = jnp.where(cc < rr, 1.0, 0.0).astype(BF16)
    rank = jnp.dot(earlier, named, preferred_element_type=F32)
    fits = rank == (i & 3).astype(F32)
    return first & fits, second & fits


def prep_body(rows_hbm, picks_ref, weight_ref, gain_ref, out_ref, w_ref, rows, sem):
    _, _, y, c = where_am_i()
    copy = pltpu.make_async_copy(rows_hbm.at[pl.ds(y * 64, 64)], rows, sem)
    copy.start()
    first, second = slot_matrix(picks_ref[...], c)
    weights = weight_ref[...]
    w_ref[...] = jnp.where(first, weights[:, 0:1], 0.0) + jnp.where(second, weights[:, 1:2], 0.0)
    select = jnp.where(first | second, 1.0, 0.0).astype(BF16)
    copy.wait()
    wide = rows[...].astype(F32)
    scale = lax.rsqrt(jnp.mean(wide * wide, axis=-1, keepdims=True) + 1e-6)
    step = 512
    for n in range(0, D, step):
        normed = (wide[:, n : n + step] * scale * gain_ref[:, n : n + step]).astype(BF16)
        got = lax.dot_general(select, normed, TN, preferred_element_type=F32)
        out_ref[:, :, n : n + step] = got.reshape(16, 8, step).astype(BF16)


def prep(rows, picks, weights, gain):
    return pl.pallas_call(
        prep_body,
        out_shape=(jax.ShapeDtypeStruct((16, 8, D), BF16), jax.ShapeDtypeStruct((64, 128), F32)),
        in_specs=[pl.BlockSpec(memory_space=pl.ANY)] + [pl.BlockSpec(memory_space=pltpu.VMEM)] * 3,
        out_specs=[pl.BlockSpec(memory_space=pltpu.VMEM)] * 2,
        scratch_shapes=[pltpu.VMEM((64, D), BF16), pltpu.SemaphoreType.DMA],
        compiler_params=pltpu.CompilerParams(vmem_limit_bytes=VLIM),
        name="prep",
    )(rows, picks, weights, gain)


def rates(logit):
    rate = (jnp.minimum(logit, 0.0) - jnp.log1p(jnp.exp(-jnp.abs(logit)))) * (1.0 / 16.0)
    hi = rate.astype(BF16)
    rest = rate - hi.astype(F32)
    mid = rest.astype(BF16)
    low = (rest - mid.astype(F32)).astype(BF16)
    rr = lax.broadcasted_iota(jnp.int32, (BLK, BLK), 0)
    cc = lax.broadcasted_iota(jnp.int32, (BLK, BLK), 1)
    lower = jnp.where(cc <= rr, 1.0, 0.0).astype(BF16)
    cum = jnp.dot(lower, low, preferred_element_type=F32)
    cum = cum + jnp.dot(lower, mid, preferred_element_type=F32)
    return cum + jnp.dot(lower, hi, preferred_element_type=F32)


def pass_a(k_ref, v_ref, g_ref, st_ref, tot_ref):
    st_ref[...] = jnp.zeros_like(st_ref)
    tot_ref[...] = jnp.zeros_like(tot_ref)

    def block(n, carry):
        at = pl.ds(n * BLK, BLK)
        cum = rates(g_ref[at, :])
        end = cum[BLK - 1 : BLK, :]
        to_end = (k_ref[at, :].astype(F32) * jnp.exp(end - cum)).astype(BF16)
        decay = jnp.exp(end)
        values = v_ref[at, :]
        for h in range(2):
            update = lax.dot_general(
                values[:, h * DV : (h + 1) * DV],
                to_end[:, h * DK : (h + 1) * DK],
                TN,
                preferred_element_type=F32,
            )
            st_ref[h] = st_ref[h] * decay[:, h * DK : (h + 1) * DK] + update
        tot_ref[...] = tot_ref[...] + end
        return carry

    lax.fori_loop(0, 16, block, 0)


def pass_b_block(n, q_ref, k_ref, v_ref, g_ref, gain_ref, st_ref, out_ref):
    at = pl.ds(pl.multiple_of(n * BLK, BLK), BLK)
    cum = rates(g_ref[at, :])
    end = cum[BLK - 1 : BLK, :]
    keys = k_ref[at, :].astype(F32)
    query_decay = (q_ref[at, :].astype(F32) * jnp.exp(cum)).astype(BF16)
    key_decay = (keys * jnp.exp(-cum)).astype(BF16)
    to_end = (keys * jnp.exp(end - cum)).astype(BF16)
    decay = jnp.exp(end)
    values = v_ref[at, :]
    rr = lax.broadcasted_iota(jnp.int32, (BLK, BLK), 0)
    cc = lax.broadcasted_iota(jnp.int32, (BLK, BLK), 1)
    for h in range(2):
        ks, vs = slice(h * DK, (h + 1) * DK), slice(h * DV, (h + 1) * DV)
        scores = lax.dot_general(query_decay[:, ks], key_decay[:, ks], NT, preferred_element_type=F32)
        weights = jnp.where(cc <= rr, scores, 0.0).astype(BF16)
        state = st_ref[h]
        total = jnp.dot(weights, values[:, vs], preferred_element_type=F32) + lax.dot_general(
            query_decay[:, ks], state.astype(BF16), NT, preferred_element_type=F32
        )
        scale = lax.rsqrt(jnp.mean(total * total, axis=-1, keepdims=True) + 1e-6)
        out_ref[at, vs] = (total * scale * gain_ref[...]).astype(BF16)
        update = lax.dot_general(values[:, vs], to_end[:, ks], TN, preferred_element_type=F32)
        st_ref[h] = state * decay[:, ks] + update


def k1_body(
    out_hbm, k_ref, v_ref, g_ref, arr, inc,
    st, tot, xs, xr, zs_buf, zr, acc, pbuf,
    a_send, a_recv, y_send, y_recv, f_send, p_send, p_recv,
    x1_send, x1_recv, z_send, z_recv, x2_send, x2_recv,
):
    z, x, y, c = where_am_i()
    up, down, far = lax.rem(y + 1, NY), lax.rem(y + NY - 1, NY), lax.rem(y + 2, NY)
    xpar, xhalf = lax.rem(x, 2), x // 2
    groups = exchange_peers(z, x, y, c) + tp_peers(y, c)
    groups += [({"x": lax.rem(x + d, NX)}, True) for d in range(1, NX)]
    groups += [({"z": lax.rem(z + d, NZ)}, True) for d in range(1, NZ)]
    greet(groups)

    def is_self(zd, xd):
        return (zd == z) & (xd == x) & (xpar == c)

    def exchange(j, xh):
        zd, xd = near(z, j), 2 * xh + c
        return is_self(zd, xd), remote(
            out_hbm.at[zd * 2 + xh],
            arr.at[xpar, y, z, xhalf],
            a_send.at[zd, xh],
            a_recv.at[z],
            z=zd,
            x=xd,
            y=y,
            c=xpar,
        )

    def send_out(j, carry):
        for xh in range(2):
            own, copy = exchange(j, xh)

            @pl.when(own)
            def _():
                pltpu.make_async_copy(out_hbm.at[z * 2 + xhalf], arr.at[c, y, z, xhalf], a_recv.at[z]).start()

            @pl.when(jnp.logical_not(own))
            def _():
                copy.start()

        return carry

    lax.fori_loop(0, NZ, send_out, 0)

    pass_a(k_ref, v_ref, g_ref, st, tot)
    dec = jnp.exp(tot[...])
    for h in range(2):
        row = jnp.broadcast_to(dec[:, h * DK : (h + 1) * DK], (8, DK))
        hi = row.astype(BF16)
        low = (row - hi.astype(F32)).astype(BF16)
        for part in range(4):
            xs[part, h, 0:64, :] = st[h, part * 64 : (part + 1) * 64, :].astype(BF16)
            xs[part, h, 64:72, :] = hi
            xs[part, h, 72:80, :] = low
    xr[x] = xs[x]

    def x1(d):
        xd = lax.rem(x + d, NX)
        return remote(xs.at[xd], xr.at[x], x1_send.at[d - 1], x1_recv.at[x], x=xd)

    for d in range(1, NX):
        x1(d).start()

    def own_copies(j):
        s = near(z, j)
        piece = arr.at[c, y, s]
        return [
            remote(piece, piece, y_send.at[0, s], y_recv.at[y, s], y=up),
            remote(piece, piece, y_send.at[1, s], y_recv.at[y, s], y=down),
            remote(piece, piece, p_send.at[y, s], p_recv.at[y, s], c=1 - c),
        ]

    def to_partner(ysrc, s):
        piece = arr.at[c, ysrc, s]
        return remote(piece, piece, p_send.at[ysrc, s], p_recv.at[ysrc, s], c=1 - c)

    def onward(ysrc, s, ydst):
        piece = arr.at[c, ysrc, s]
        return remote(piece, piece, f_send.at[s], y_recv.at[ysrc, s], y=ydst)

    def gather_step(i, carry):
        @pl.when(i < NZ)
        def _():
            s = near(z, i)
            await_bytes(arr.at[c, y, s], a_recv.at[s])
            for copy in own_copies(i):
                copy.start()

        @pl.when((i >= 1) & (i < NZ + 1))
        def _():
            j = i - 1
            s = near(z, j)
            await_bytes(arr.at[c, down, s], y_recv.at[down, s])

            @pl.when(lax.rem(j, 2) == 0)
            def _():
                onward(down, s, up).start()

            to_partner(down, s).start()
            await_bytes(arr.at[c, up, s], y_recv.at[up, s])

            @pl.when(lax.rem(j, 2) == 1)
            def _():
                onward(up, s, down).start()

            to_partner(up, s).start()

        @pl.when(i >= 2)
        def _():
            s = near(z, i - 2)
            await_bytes(arr.at[c, far, s], y_recv.at[far, s])
            to_partner(far, s).start()

        return carry

    lax.fori_loop(0, 6, gather_step, 0)

    for d in range(1, NX):
        src = lax.rem(x + d, NX)
        await_bytes(xr.at[src], x1_recv.at[src])

    def part_of(buf, at, h):
        piece = buf[at, h].astype(F32)
        return piece[0:64, :], piece[64:65, :] + piece[72:73, :]

    for h in range(2):
        state, decay = part_of(xr, 0, h)
        for k in range(1, NX):
            s_k, d_k = part_of(xr, k, h)
            state = state * d_k + s_k
            decay = decay * d_k
        row = jnp.broadcast_to(decay, (8, DK))
        hi = row.astype(BF16)
        zs_buf[h, 0:64, :] = state.astype(BF16)
        zs_buf[h, 64:72, :] = hi
        zs_buf[h, 72:80, :] = (row - hi.astype(F32)).astype(BF16)

    def z_copy(zd):
        return remote(zs_buf, zr.at[z], z_send.at[zd], z_recv.at[z], z=zd)

    for zd in range(1, NZ):

        @pl.when(zd > z)
        def _(zd=zd):
            z_copy(zd).start()

    lax.fori_loop(6, NZ + 2, gather_step, 0)

    acc[...] = jnp.zeros_like(acc)
    for zsrc in range(NZ - 1):

        @pl.when(zsrc < z)
        def _(zsrc=zsrc):
            await_bytes(zr.at[zsrc], z_recv.at[zsrc])
            for h in range(2):
                s_k, d_k = part_of(zr, zsrc, h)
                acc[h] = acc[h] * d_k + s_k

    for h in range(2):
        state = acc[h]
        for k in range(NX):
            pbuf[k, h] = state
            s_k, d_k = part_of(xr, k, h)
            state = state * d_k + s_k
    inc[x] = pbuf[x]

    def x2(d):
        xd = lax.rem(x + d, NX)
        return remote(pbuf.at[xd], inc.at[x], x2_send.at[d - 1], x2_recv.at[x], x=xd)

    for d in range(1, NX):
        x2(d).start()

    def finish(j, carry):
        for xh in range(2):
            own, copy = exchange(j, xh)

            @pl.when(jnp.logical_not(own))
            def _():
                copy.wait_send()

        s = near(z, j)
        for copy in own_copies(j)[:2]:
            copy.wait_send()

        @pl.when(lax.rem(j, 2) == 0)
        def _():
            onward(down, s, up).wait_send()

        @pl.when(lax.rem(j, 2) == 1)
        def _():
            onward(up, s, down).wait_send()

        for ysrc in range(NY):
            to_partner(ysrc, s).wait_send()
            await_bytes(arr.at[1 - c, ysrc, s], p_recv.at[ysrc, s])
        return carry

    lax.fori_loop(0, NZ, finish, 0)
    for zd in range(1, NZ):

        @pl.when(zd > z)
        def _(zd=zd):
            z_copy(zd).wait_send()

    for d in range(1, NX):
        x1(d).wait_send()
        x2(d).wait_send()
        src = lax.rem(x + d, NX)
        await_bytes(inc.at[src], x2_recv.at[src])


def k1(outgoing, k, v, g):
    dma = pltpu.SemaphoreType.DMA
    vmem = pl.BlockSpec(memory_space=pltpu.VMEM)
    return pl.pallas_call(
        k1_body,
        out_shape=(
            jax.ShapeDtypeStruct((2, NY, NZ, 2, 8, D), BF16),
            jax.ShapeDtypeStruct((4, 2, 64, DK), F32),
        ),
        in_specs=[pl.BlockSpec(memory_space=pl.ANY), vmem, vmem, vmem],
        out_specs=[vmem, vmem],
        scratch_shapes=[
            pltpu.VMEM((2, DV, DK), F32),
            pltpu.VMEM((1, 2 * DK), F32),
            pltpu.VMEM((4, 2, 80, DK), BF16),
            pltpu.VMEM((4, 2, 80, DK), BF16),
            pltpu.VMEM((2, 80, DK), BF16),
            pltpu.VMEM((NZ, 2, 80, DK), BF16),
            pltpu.VMEM((2, 64, DK), F32),
            pltpu.VMEM((4, 2, 64, DK), F32),
            dma((NZ, 2)), dma((NZ,)), dma((2, NZ)), dma((NY, NZ)), dma((NZ,)), dma((NY, NZ)), dma((NY, NZ)),
            dma((3,)), dma((4,)), dma((NZ,)), dma((NZ,)), dma((3,)), dma((4,)),
        ],
        compiler_params=pltpu.CompilerParams(collective_id=0, has_side_effects=True, vmem_limit_bytes=VLIM),
        name="dispatch",
    )(outgoing, k, v, g)


def ffn_body(x_ref, gate_ref, up_ref, down_ref, o_ref):
    rows = x_ref[...]
    gate = jnp.dot(rows, gate_ref[...], preferred_element_type=F32)
    up = jnp.dot(rows, up_ref[...], preferred_element_type=F32)
    hidden = (gate / (1.0 + jnp.exp(-gate)) * up).astype(BF16)
    step = 1024
    for n in range(0, D, step):
        o_ref[:, n : n + step] = jnp.dot(
            hidden, down_ref[:, n : n + step], preferred_element_type=F32
        ).astype(BF16)


def ffn(rows, gate, up, down):
    tile = 256
    width = gate.shape[1]
    return pl.pallas_call(
        ffn_body,
        grid=(rows.shape[0] // tile,),
        out_shape=jax.ShapeDtypeStruct(rows.shape, BF16),
        in_specs=[
            pl.BlockSpec((tile, D), lambda i: (i, 0)),
            pl.BlockSpec((D, width), lambda i: (0, 0)),
            pl.BlockSpec((D, width), lambda i: (0, 0)),
            pl.BlockSpec((width, D), lambda i: (0, 0)),
        ],
        out_specs=pl.BlockSpec((tile, D), lambda i: (i, 0)),
        compiler_params=pltpu.CompilerParams(vmem_limit_bytes=VLIM),
        name="expert",
    )(rows, gate, up, down)


def k3_body(
    part, w_ref, post_ref, q_ref, k_ref, v_ref, g_ref, gain_ref, inc_ref, mixed, routed,
    r1, low, upd, fin, ret, st, mine, cs, cr,
    d_send, d_recv, l_send, l_recv, t_send, u_send, u_recv, b_send, b_recv, c_send, c_recv,
):
    z, x, y, c = where_am_i()
    up, down, far = lax.rem(y + 1, NY), lax.rem(y + NY - 1, NY), lax.rem(y + 2, NY)
    xpar, xhalf = lax.rem(x, 2), x // 2
    greet(exchange_peers(z, x, y, c) + tp_peers(y, c))

    def over(j):
        s = near(z, j)
        return remote(part.at[1 - c, :, s], r1.at[:, s], d_send.at[s], d_recv.at[s], c=1 - c)

    def start_over(j, carry):
        over(j).start()
        return carry

    lax.fori_loop(0, NZ, start_over, 0)

    for h in range(2):
        for part_no in range(4):
            st[h, part_no * 64 : (part_no + 1) * 64, :] = inc_ref[part_no, h]

    def relay(j, to):
        s = near(z, j)
        return remote(r1.at[far, s], low.at[s], l_send.at[s], l_recv.at[s], y=to)

    def direct(j, to, side):
        s = near(z, j)
        return remote(r1.at[to, s], upd.at[side, s], u_send.at[s], u_recv.at[side, s], y=to)

    def joined(j, to, side):
        s = near(z, j)
        return remote(r1.at[to, s], upd.at[side, s], t_send.at[s], u_recv.at[side, s], y=to)

    def back(j, xh):
        s = near(z, j)
        xd = 2 * xh + c
        own = (s == z) & (xd == x) & (xpar == c)
        return own, remote(
            fin.at[s, xh],
            ret.at[z, xhalf],
            b_send.at[s, xh],
            b_recv.at[z, xhalf],
            z=s,
            x=xd,
            y=y,
            c=xpar,
        )

    def step(i, carry):
        @pl.when(i < NZ)
        def _():
            j = i
            s = near(z, j)
            even = lax.rem(j, 2) == 0
            await_bytes(r1.at[:, s], d_recv.at[s])

            def add(yy, inner):
                for xh in range(2):
                    r1[yy, s, xh] = (r1[yy, s, xh].astype(F32) + part[c, yy, s, xh].astype(F32)).astype(BF16)
                return inner

            lax.fori_loop(0, NY, add, 0)

            @pl.when(even)
            def _():
                relay(j, down).start()
                direct(j, up, 0).start()

            @pl.when(jnp.logical_not(even))
            def _():
                relay(j, up).start()
                direct(j, down, 1).start()

            for half in range(2):
                pass_b_block(2 * i + half, q_ref, k_ref, v_ref, g_ref, gain_ref, st, mixed)

        @pl.when((i >= 1) & (i < NZ + 1))
        def _():
            j = i - 1
            s = near(z, j)
            even = lax.rem(j, 2) == 0
            await_bytes(low.at[s], l_recv.at[s])
            to = jnp.where(even, down, up)
            for xh in range(2):
                r1[to, s, xh] = (r1[to, s, xh].astype(F32) + low[s, xh].astype(F32)).astype(BF16)

            @pl.when(even)
            def _():
                joined(j, down, 1).start()

            @pl.when(jnp.logical_not(even))
            def _():
                joined(j, up, 0).start()

        @pl.when(i >= 2)
        def _():
            j = i - 2
            s = near(z, j)
            for side in range(2):
                await_bytes(upd.at[side, s], u_recv.at[side, s])
            for xh in range(2):
                total = r1[y, s, xh].astype(F32) + upd[0, s, xh].astype(F32) + upd[1, s, xh].astype(F32)
                fin[s, xh] = total.astype(BF16)
                own, copy = back(j, xh)

                @pl.when(own)
                def _(xh=xh):
                    ret[s, xh] = fin[s, xh]

                @pl.when(jnp.logical_not(own))
                def _(copy=copy):
                    copy.start()

        return carry

    lax.fori_loop(0, NZ + 2, step, 0)

    def finish(j, carry):
        s = near(z, j)
        for xh in range(2):
            own, copy = back(j, xh)

            @pl.when(jnp.logical_not(own))
            def _(copy=copy, xh=xh):
                copy.wait_send()
                await_bytes(ret.at[s, xh], b_recv.at[s, xh])

        over(j).wait_send()
        await_bytes(low.at[s], l_send.at[s])
        await_bytes(low.at[s], u_send.at[s])
        await_bytes(low.at[s], t_send.at[s])
        return carry

    lax.fori_loop(0, NZ, finish, 0)

    weights = w_ref[...]
    w_hi = weights.astype(BF16)
    w_low = (weights - w_hi.astype(F32)).astype(BF16)
    width = 512

    def weigh(n, carry):
        at = pl.ds(pl.multiple_of(n * width, width), width)
        rows = ret[:, :, :, at].astype(F32).reshape(128, width).astype(BF16)
        got = jnp.dot(w_hi, rows, preferred_element_type=F32) + jnp.dot(w_low, rows, preferred_element_type=F32)
        mine[:, at] = jnp.where(c == 0, got[0:32], got[32:64])
        cs[:, at] = jnp.where(c == 0, got[32:64], got[0:32])
        return carry

    lax.fori_loop(0, D // width, weigh, 0)
    swap = remote(cs, cr, c_send, c_recv, c=1 - c)
    swap.start()
    swap.wait()
    total = mine[...] + cr[...]
    scale = lax.rsqrt(jnp.mean(total * total, axis=-1, keepdims=True) + 1e-6)
    routed[...] = (total * scale * post_ref[...]).astype(BF16)


def k3(part, w, post, q, k, v, g, gain, inc):
    dma = pltpu.SemaphoreType.DMA
    vmem = pl.BlockSpec(memory_space=pltpu.VMEM)
    return pl.pallas_call(
        k3_body,
        out_shape=(
            jax.ShapeDtypeStruct((1024, 2 * DV), BF16),
            jax.ShapeDtypeStruct((32, D), BF16),
        ),
        in_specs=[vmem] * 9,
        out_specs=[vmem, vmem],
        scratch_shapes=[
            pltpu.VMEM((NY, NZ, 2, 8, D), BF16),
            pltpu.VMEM((NZ, 2, 8, D), BF16),
            pltpu.VMEM((2, NZ, 2, 8, D), BF16),
            pltpu.VMEM((NZ, 2, 8, D), BF16),
            pltpu.VMEM((NZ, 2, 8, D), BF16),
            pltpu.VMEM((2, DV, DK), F32),
            pltpu.VMEM((32, D), F32),
            pltpu.VMEM((32, D), F32),
            pltpu.VMEM((32, D), F32),
            dma((NZ,)), dma((NZ,)), dma((NZ,)), dma((NZ,)), dma((NZ,)), dma((NZ,)), dma((2, NZ)),
            dma((NZ, 2)), dma((NZ, 2)), dma(()), dma(()),
        ],
        compiler_params=pltpu.CompilerParams(collective_id=1, has_side_effects=True, vmem_limit_bytes=VLIM),
        name="combine",
    )(part, w, post, q, k, v, g, gain, inc)


def on_device(
    queries,
    key_vectors,
    value_vectors,
    decay_logit,
    head_gain,
    routed_rows,
    pre_gain,
    expert_pick,
    route_weight,
    gate_weight,
    up_weight,
    down_weight,
    post_gain,
):
    y = lax.axis_index("y")
    picks = lax.dynamic_slice_in_dim(expert_pick, y * 64, 64, 0)
    weights = lax.dynamic_slice_in_dim(route_weight, y * 64, 64, 0)
    outgoing, w = prep(routed_rows, picks, weights, pre_gain.reshape(1, D))
    arrived, incoming = k1(outgoing, key_vectors, value_vectors, decay_logit)
    part = ffn(arrived.reshape(1024, D), gate_weight[0], up_weight[0], down_weight[0])
    return k3(
        part.reshape(arrived.shape),
        w,
        post_gain.reshape(1, D),
        queries,
        key_vectors,
        value_vectors,
        decay_logit,
        head_gain.reshape(1, DV),
        incoming,
    )


def solution(mesh):
    torus = Mesh(mesh.devices.reshape(NZ, NX, NY, 2), ("z", "x", "y", "c"))
    placed = (
        P(EP, TP),
        P(EP, TP),
        P(EP, TP),
        P(EP, TP),
        P(),
        P(EP, None),
        P(),
        P(EP, None),
        P(EP, None),
        P(EP, None, TP),
        P(EP, None, TP),
        P(EP, TP, None),
        P(),
    )
    return jax.shard_map(
        on_device,
        mesh=torus,
        in_specs=placed,
        out_specs=(P(EP, TP), P(EP + TP, None)),
        check_vma=False,
    )
```

time: 292 us -> 161 us (0.55)
  Pallas kernels: 0 us -> 151 us
  blocking collectives: 96.7 us -> 0 us
  other arithmetic: 50.4 us -> 0 us
  local copies, waits for them, and re-layouts: 52.1 us -> 5.92 us
  waiting for transfers between devices: 36.4 us -> 0 us
  matrix products: 25.8 us -> 0 us
  between operations: 15.9 us -> 0.68 us
  starting transfers between devices: 9.97 us -> 0 us
    pallas_call x0 -> x4, Pallas kernels: none -> 151 us  [the longest x1 67.4 us: k3(): pl.pallas_call(k3_body, out_shape=(jax.ShapeDtypeStruct((1024, 2 * DV), B...]
    all_gather x3 -> x0, blocking collectives: 58.7 us -> none  [prefix_by_axis(): lax.all_gather(part.astype(kind), axis)]
    all_to_all x1 -> x0, blocking collectives: 38 us -> none  [routed_experts(): lax.all_to_all(outgoing, EP, split_axis=1, concat_axis=1, tiled=True)]
    all_gather x2 -> x0, waiting for transfers between devices: 33.6 us -> none  [the longest x1 33.6 us: routed_experts(): lax.all_gather(lax.all_to_all(outgoing, EP, split_axis=1, concat_axis=1,...]
    dot_general x6 -> x0, matrix products: 25.8 us -> none  [the longest x1 6.46 us: routed_experts(): jnp.einsum('pskd,df->pskf', arrived, gate_local, preferred_element_type=j...]
    scatter x1 -> x0, local copies, waits for them, and re-layouts: 22.1 us -> none  [routed_experts(): table = jnp.full((tp_count, experts * capacity), ep_rows, jnp.int32).at[s...]
    add x18 -> x0, other arithmetic: 17.2 us -> none  [the longest x16 17.1 us: advance(): carry_state * block_decay[..., None] + block_update]
    dynamic_update_slice x32 -> x0, other arithmetic: 11.8 us -> none  [token_mixer(): lax.scan(advance, start_carry, (update, step_decay))]
  transfers between devices with their start and end apart: 4 -> 0, of which waited for: 2 -> 0; matrix products, arithmetic and copies ran while one was open for 23% -> 0% of each run, Pallas kernels for 0% -> 0%
where the time goes in v1:
time: 161 us; the launch traced here: 158 us
  Pallas kernels  151 us (94%)
  local copies, waits for them, and re-layouts  5.92 us (4%)
    pallas_call x1, Pallas kernels, k3(): pl.pallas_call(k3_body, out_shape=(jax.ShapeDtypeStruct((1024, 2 * DV), B...  67.4 us
    pallas_call x1, Pallas kernels, k1(): pl.pallas_call(k1_body, out_shape=(jax.ShapeDtypeStruct((2, NY, NZ, 2, 8,...  67.2 us
    pallas_call x1, Pallas kernels, ffn(): pl.pallas_call(ffn_body, grid=(rows.shape[0] // tile,), out_shape=jax.Sha...  13.1 us
    unnamed x8, local copies, waits for them, and re-layouts  5.1 us
    pallas_call x1, Pallas kernels, prep(): pl.pallas_call(prep_body, out_shape=(jax.ShapeDtypeStruct((16, 8, D), BF1...  3.43 us

profile of v1, /device:TPU:1, one launch (start us, length us, event | category | flops | bytes accessed | tf_op | source)
XLA Modules:
  0.0 157.7 jit_solution(5366293758352268369)
XLA Ops:
  0.6 0.0 copy-start
  0.6 0.7 copy-done
  1.3 0.1 constant_dynamic-slice_fusion.1
  1.4 0.7 constant_dynamic-slice_fusion
  2.1 0.7 copy.18.weight_ref
  2.8 0.7 copy.17.picks_ref
  3.6 3.4 %prep.1 = (bf16[16,8,4096]{2,1,0:T(8,128)(2,1)}, f32[64,128]{1,0:T(8,128)}) custom-call(bf16[256,4096]{1,0:T(8,128)(2,1)} %rows_hbm.1, s32[64,2]{1,0:T(8,128)} %copy.17.picks_ref, f32[64,2]{1,0:T(8,128)} %copy.18.weight_ref, f32[1,4096]{1,0:T(1,128)} %bitcast.13), custom_call_target="tpu_custom_call" | custom-call | tf_op jit(solution)/shard_map/prep/pallas_call | solution.py:110
  7.0 67.2 %dispatch.1 = (bf16[2,4,8,2,8,4096]{5,4,3,2,1,0:T(8,128)(2,1)}, f32[4,2,64,128]{3,2,1,0:T(8,128)}) custom-call(bf16[16,8,4096]{2,1,0:T(8,128)(2,1)} %get-tuple-element.6.out_hbm, bf16[1024,256]{1,0:T(8,128)(2,1)} %k_ref.3, bf16[1024,512]{1,0:T(8,128)(2,1)} %v_ref.3, f32[1024,256]{1,0:T(8,128)} %g_ref.3), custom_call_target="tpu_custom_call" | custom-call | tf_op jit(solution)/shard_map/dispatch/pallas_call | solution.py:403
  74.2 13.1 %expert.1 = bf16[1024,4096]{1,0:T(8,128)(2,1)} custom-call(bf16[1024,4096]{1,0:T(8,128)(2,1)} %bitcast.9, bf16[4096,256]{1,0:T(8,128)(2,1)} %bitcast.10, bf16[4096,256]{1,0:T(8,128)(2,1)} %bitcast.11, bf16[256,4096]{1,0:T(8,128)(2,1)} %bitcast.12), custom_call_target="tpu_custom_call" | custom-call | tf_op jit(solution)/shard_map/expert/pallas_call | solution.py:443
  87.3 67.4 %combine.1 = (bf16[1024,512]{1,0:T(8,128)(2,1)}, bf16[32,4096]{1,0:T(8,128)(2,1)}) custom-call(bf16[2,4,8,2,8,4096]{5,4,3,2,1,0:T(8,128)(2,1)} %bitcast.8, f32[64,128]{1,0:T(8,128)} %get-tuple-element.8.w_ref, f32[1,4096]{1,0:T(1,128)} %bitcast.14, bf16[1024,256]{1,0:T(8,128)(2,1)} %q_ref.1, bf16[1024,256]{1,0:T(8,128)(2,1)} %k_ref.3, ...), custom_call_target="tpu_custom_call" | custom-call | tf_op jit(solution)/shard_map/combine/pallas_call | solution.py:622
  154.7 0.0 copy-start.1
  154.7 2.3 %copy.21 = bf16[1024,512]{1,0:T(8,128)(2,1)} copy(bf16[1024,512]{1,0:T(8,128)(2,1)} %get-tuple-element.12) | data formatting | bytes 2097152
  157.0 0.0 copy-done.1
  157.0 0.7 copy.22
Async XLA Ops:
  0.6 0.7 copy-start
  154.7 2.3 %copy-start.1 = (bf16[32,4096]{1,0:T(8,128)(2,1)S(1)}, bf16[32,4096]{1,0:T(8,128)(2,1)}, u32[]{:S(2)}) copy-start(bf16[32,4096]{1,0:T(8,128)(2,1)} %get-tuple-element.13) | copy-start | bytes 786436

commit v2 on v1

v2 whole, which is shorter than its diff:
```python
import jax
import jax.numpy as jnp
from jax import lax
from jax.experimental import pallas as pl
from jax.experimental.pallas import tpu as pltpu
from jax.sharding import Mesh
from jax.sharding import PartitionSpec as P

BLK, DK, DV = 64, 128, 256
NZ, NX, NY = 8, 4, 4
D = 4096
MESH = pl.DeviceIdType.MESH
EP, TP = ("z", "x"), ("y", "c")
F32, BF16 = jnp.float32, jnp.bfloat16
VLIM = 60 * 1024 * 1024
NT = (((1,), (1,)), ((), ()))
TN = (((0,), (0,)), ((), ()))


def where_am_i():
    return tuple(lax.axis_index(a) for a in ("z", "x", "y", "c"))


def near(z, j):
    off = jnp.where(lax.rem(j, 2) == 1, (j + 1) // 2, NZ - j // 2)
    return lax.rem(z + off, NZ)


def remote(src, dst, ssem, rsem, **to):
    return pltpu.make_async_remote_copy(
        src_ref=src, dst_ref=dst, send_sem=ssem, recv_sem=rsem, device_id=to, device_id_type=MESH
    )


def await_bytes(ref, sem):
    pltpu.make_async_copy(ref, ref, sem).wait()


def greet(groups):
    barrier = pltpu.get_barrier_semaphore()
    total = 0
    for to, is_other in groups:
        if is_other is True:
            pl.semaphore_signal(barrier, inc=1, device_id=to, device_id_type=MESH)
            total = total + 1
        else:

            @pl.when(is_other)
            def _(to=to):
                pl.semaphore_signal(barrier, inc=1, device_id=to, device_id_type=MESH)

            total = total + is_other.astype(jnp.int32)
    return barrier, total


def exchange_peers(z, x, y, c):
    peers = []
    for dz in range(NZ):
        for xh in range(2):
            zd, xd = lax.rem(z + dz, NZ), 2 * xh + c
            to = {"z": zd, "x": xd, "y": y, "c": lax.rem(x, 2)}
            peers.append((to, True if dz else jnp.logical_not((xd == x) & (lax.rem(x, 2) == c))))
    return peers


def tp_peers(y, c):
    return [
        ({"y": lax.rem(y + 1, NY)}, True),
        ({"y": lax.rem(y + NY - 1, NY)}, True),
        ({"c": 1 - c}, True),
    ]


def quarter(row, y):
    parts = [row[:, k * 64 : (k + 1) * 64] for k in range(4)]
    return jnp.where(y == 0, parts[0], jnp.where(y == 1, parts[1], jnp.where(y == 2, parts[2], parts[3])))


def slot_matrices(first_pick, second_pick, c):
    shape = (128, 64)
    i = lax.broadcasted_iota(jnp.int32, shape, 0)
    r = lax.broadcasted_iota(jnp.int32, shape, 1)
    expert = 2 * (i >> 3) + c
    same_block = (r >> 5) == ((i >> 2) & 1)
    first = (first_pick == expert) & same_block
    second = (second_pick == expert) & same_block
    named = jnp.where(first | second, 1.0, 0.0).astype(BF16)
    rr = lax.broadcasted_iota(jnp.int32, (64, 64), 0)
    cc = lax.broadcasted_iota(jnp.int32, (64, 64), 1)
    earlier = jnp.where(rr < cc, 1.0, 0.0).astype(BF16)
    rank = jnp.dot(named, earlier, preferred_element_type=F32)
    fits = rank == (i & 3).astype(F32)
    return first & fits, second & fits


def rates(logit):
    rate = (jnp.minimum(logit, 0.0) - jnp.log1p(jnp.exp(-jnp.abs(logit)))) * (1.0 / 16.0)
    hi = rate.astype(BF16)
    rest = rate - hi.astype(F32)
    mid = rest.astype(BF16)
    low = (rest - mid.astype(F32)).astype(BF16)
    rr = lax.broadcasted_iota(jnp.int32, (BLK, BLK), 0)
    cc = lax.broadcasted_iota(jnp.int32, (BLK, BLK), 1)
    lower = jnp.where(cc <= rr, 1.0, 0.0).astype(BF16)
    cum = jnp.dot(lower, low, preferred_element_type=F32)
    cum = cum + jnp.dot(lower, mid, preferred_element_type=F32)
    return cum + jnp.dot(lower, hi, preferred_element_type=F32)


def pass_a(k_ref, v_ref, g_ref, st_ref, tot_ref):
    st_ref[...] = jnp.zeros_like(st_ref)
    tot_ref[...] = jnp.zeros_like(tot_ref)

    def block(n, carry):
        at = pl.ds(n * BLK, BLK)
        cum = rates(g_ref[at, :])
        end = cum[BLK - 1 : BLK, :]
        to_end = (k_ref[at, :].astype(F32) * jnp.exp(end - cum)).astype(BF16)
        decay = jnp.exp(end)
        values = v_ref[at, :]
        for h in range(2):
            update = lax.dot_general(
                values[:, h * DV : (h + 1) * DV],
                to_end[:, h * DK : (h + 1) * DK],
                TN,
                preferred_element_type=F32,
            )
            st_ref[h] = st_ref[h] * decay[:, h * DK : (h + 1) * DK] + update
        tot_ref[...] = tot_ref[...] + end
        return carry

    lax.fori_loop(0, 16, block, 0)


def pass_b_block(n, q_ref, k_ref, v_ref, g_ref, gain_ref, st_ref, out_ref):
    at = pl.ds(pl.multiple_of(n * BLK, BLK), BLK)
    cum = rates(g_ref[at, :])
    end = cum[BLK - 1 : BLK, :]
    keys = k_ref[at, :].astype(F32)
    query_decay = (q_ref[at, :].astype(F32) * jnp.exp(cum)).astype(BF16)
    key_decay = (keys * jnp.exp(-cum)).astype(BF16)
    to_end = (keys * jnp.exp(end - cum)).astype(BF16)
    decay = jnp.exp(end)
    values = v_ref[at, :]
    rr = lax.broadcasted_iota(jnp.int32, (BLK, BLK), 0)
    cc = lax.broadcasted_iota(jnp.int32, (BLK, BLK), 1)
    for h in range(2):
        ks, vs = slice(h * DK, (h + 1) * DK), slice(h * DV, (h + 1) * DV)
        scores = lax.dot_general(query_decay[:, ks], key_decay[:, ks], NT, preferred_element_type=F32)
        weights = jnp.where(cc <= rr, scores, 0.0).astype(BF16)
        state = st_ref[h]
        total = jnp.dot(weights, values[:, vs], preferred_element_type=F32) + lax.dot_general(
            query_decay[:, ks], state.astype(BF16), NT, preferred_element_type=F32
        )
        scale = lax.rsqrt(jnp.mean(total * total, axis=-1, keepdims=True) + 1e-6)
        out_ref[at, vs] = (total * scale * gain_ref[...]).astype(BF16)
        update = lax.dot_general(values[:, vs], to_end[:, ks], TN, preferred_element_type=F32)
        st_ref[h] = state * decay[:, ks] + update


LAST = NZ + 6


def body(
    picks_ref, weight_ref, pre_ref, post_ref, gain_ref,
    rows_hbm, gate_hbm, up_hbm, down_hbm, q_hbm, k_hbm, v_hbm, g_hbm,
    mixed, routed,
    rows, gate_w, up_w, down_w, q_ref, k_ref, v_ref, g_ref,
    outgoing, w_buf, arr, xb, part, r1, low, upd, fin, ret, mine, cs, cr,
    st, tot, xs, xr, zs_buf, zr, acc, pbuf, inc,
    load, a_send, a_recv, y_send, y_recv, f_send, p_send, p_recv,
    x1_send, x1_recv, z_send, z_recv, x2_send, x2_recv,
    d_send, d_recv, l_send, l_recv, t_send, u_send, u_recv, b_send, b_recv, c_send, c_recv,
):
    z, x, y, c = where_am_i()
    up, down, far = lax.rem(y + 1, NY), lax.rem(y + NY - 1, NY), lax.rem(y + 2, NY)
    xpar, xhalf = lax.rem(x, 2), x // 2
    loads = [
        pltpu.make_async_copy(src, dst, load.at[n])
        for n, (src, dst) in enumerate(
            [
                (rows_hbm.at[pl.ds(y * 64, 64)], rows),
                (k_hbm, k_ref),
                (v_hbm, v_ref),
                (g_hbm, g_ref),
                (gate_hbm, gate_w),
                (up_hbm, up_w),
                (down_hbm, down_w),
                (q_hbm, q_ref),
            ]
        )
    ]
    for copy in loads:
        copy.start()
    groups = exchange_peers(z, x, y, c) + tp_peers(y, c)
    groups += [({"x": lax.rem(x + d, NX)}, True) for d in range(1, NX)]
    groups += [({"z": lax.rem(z + d, NZ)}, True) for d in range(1, NZ)]
    barrier, signals = greet(groups)

    first, second = slot_matrices(quarter(picks_ref[0:1, :], y), quarter(picks_ref[1:2, :], y), c)
    w_buf[...] = jnp.where(first, quarter(weight_ref[0:1, :], y), 0.0) + jnp.where(
        second, quarter(weight_ref[1:2, :], y), 0.0
    )
    select = jnp.where(first | second, 1.0, 0.0).astype(BF16)
    loads[0].wait()
    wide = rows[...].astype(F32)
    scale = lax.rsqrt(jnp.mean(wide * wide, axis=-1, keepdims=True) + 1e-6)
    width = 512
    for n in range(0, D, width):
        normed = (wide[:, n : n + width] * scale * pre_ref[:, n : n + width]).astype(BF16)
        got = jnp.dot(select, normed, preferred_element_type=F32)
        outgoing[:, :, n : n + width] = got.reshape(16, 8, width).astype(BF16)
    pl.semaphore_wait(barrier, signals)

    def piece(j, xh):
        s, xd = near(z, j), 2 * xh + c
        return (s == z) & (xd == x) & (xpar == c), s, xd

    def exchange(j, xh):
        own, s, xd = piece(j, xh)
        return own, remote(
            outgoing.at[s * 2 + xh],
            arr.at[xpar, y, z, xhalf],
            a_send.at[s, xh],
            a_recv.at[z, xhalf],
            z=s,
            x=xd,
            y=y,
            c=xpar,
        )

    def send_out(j, carry):
        for xh in range(2):
            own, copy = exchange(j, xh)

            @pl.when(own)
            def _():
                arr[c, y, z, xhalf] = outgoing[z * 2 + xhalf]

            @pl.when(jnp.logical_not(own))
            def _():
                copy.start()

        return carry

    lax.fori_loop(0, NZ, send_out, 0)

    for copy in loads[1:4]:
        copy.wait()
    pass_a(k_ref, v_ref, g_ref, st, tot)
    dec = jnp.exp(tot[...])
    for h in range(2):
        row = jnp.broadcast_to(dec[:, h * DK : (h + 1) * DK], (8, DK))
        hi = row.astype(BF16)
        low_part = (row - hi.astype(F32)).astype(BF16)
        for n in range(4):
            xs[n, h, 0:64, :] = st[h, n * 64 : (n + 1) * 64, :].astype(BF16)
            xs[n, h, 64:72, :] = hi
            xs[n, h, 72:80, :] = low_part
    xr[x] = xs[x]

    def x1(d):
        xd = lax.rem(x + d, NX)
        return remote(xs.at[xd], xr.at[x], x1_send.at[d - 1], x1_recv.at[x], x=xd)

    def x2(d):
        xd = lax.rem(x + d, NX)
        return remote(pbuf.at[xd], inc.at[x], x2_send.at[d - 1], x2_recv.at[x], x=xd)

    def z_copy(zd):
        return remote(zs_buf, zr.at[z], z_send.at[zd], z_recv.at[z], z=zd)

    for d in range(1, NX):
        x1(d).start()

    def state_and_decay(buf, at, h):
        got = buf[at, h].astype(F32)
        return got[0:64, :], got[64:65, :] + got[72:73, :]

    def join_row():
        for d in range(1, NX):
            src = lax.rem(x + d, NX)
            await_bytes(xr.at[src], x1_recv.at[src])
        for h in range(2):
            state, decay = state_and_decay(xr, 0, h)
            for k in range(1, NX):
                s_k, d_k = state_and_decay(xr, k, h)
                state = state * d_k + s_k
                decay = decay * d_k
            row = jnp.broadcast_to(decay, (8, DK))
            hi = row.astype(BF16)
            zs_buf[h, 0:64, :] = state.astype(BF16)
            zs_buf[h, 64:72, :] = hi
            zs_buf[h, 72:80, :] = (row - hi.astype(F32)).astype(BF16)
        for zd in range(1, NZ):

            @pl.when(zd > z)
            def _(zd=zd):
                z_copy(zd).start()

    def join_planes():
        acc[...] = jnp.zeros_like(acc)
        for zsrc in range(NZ - 1):

            @pl.when(zsrc < z)
            def _(zsrc=zsrc):
                await_bytes(zr.at[zsrc], z_recv.at[zsrc])
                for h in range(2):
                    s_k, d_k = state_and_decay(zr, zsrc, h)
                    acc[h] = acc[h] * d_k + s_k

        for h in range(2):
            state = acc[h]
            for k in range(NX):
                pbuf[k, h] = state
                s_k, d_k = state_and_decay(xr, k, h)
                state = state * d_k + s_k
        inc[x] = pbuf[x]
        for d in range(1, NX):
            x2(d).start()

    def take_state():
        for d in range(1, NX):
            src = lax.rem(x + d, NX)
            await_bytes(inc.at[src], x2_recv.at[src])
        for h in range(2):
            for n in range(4):
                st[h, n * 64 : (n + 1) * 64, :] = inc[n, h]
        loads[7].wait()

    def own_copies(s):
        here = arr.at[c, y, s]
        return [
            remote(here, here, y_send.at[0, s], y_recv.at[y, s], y=up),
            remote(here, here, y_send.at[1, s], y_recv.at[y, s], y=down),
        ]

    def to_partner(ysrc, s):
        here = arr.at[c, ysrc, s]
        return remote(here, here, p_send.at[ysrc, s], p_recv.at[ysrc, s], c=1 - c)

    def onward(ysrc, s, ydst):
        here = arr.at[c, ysrc, s]
        return remote(here, here, f_send.at[s], y_recv.at[ysrc, s], y=ydst)

    def over(s):
        return remote(part.at[1 - c, :, s], r1.at[:, s], d_send.at[s], d_recv.at[s], c=1 - c)

    def relay(s, to):
        return remote(r1.at[far, s], low.at[s], l_send.at[s], l_recv.at[s], y=to)

    def direct(s, to, side):
        return remote(r1.at[to, s], upd.at[side, s], u_send.at[s], u_recv.at[side, s], y=to)

    def joined(s, to, side):
        return remote(r1.at[to, s], upd.at[side, s], t_send.at[s], u_recv.at[side, s], y=to)

    def back(j, xh):
        own, s, xd = piece(j, xh)
        return own, remote(
            fin.at[s, xh],
            ret.at[z, xhalf],
            b_send.at[s, xh],
            b_recv.at[z, xhalf],
            z=s,
            x=xd,
            y=y,
            c=xpar,
        )

    def expert(s):
        def pack(n, carry):
            at = pl.ds(pl.multiple_of(n * width, width), width)
            xb[:, at] = arr[:, :, s, :, :, at].astype(F32).reshape(128, width).astype(BF16)
            return carry

        lax.fori_loop(0, D // width, pack, 0)
        gate = jnp.dot(xb[...], gate_w[...], preferred_element_type=F32)
        above = jnp.dot(xb[...], up_w[...], preferred_element_type=F32)
        hidden = (gate / (1.0 + jnp.exp(-gate)) * above).astype(BF16)

        def out(n, carry):
            at = pl.ds(pl.multiple_of(n * width, width), width)
            got = jnp.dot(hidden, down_w[:, at], preferred_element_type=F32)
            part[:, :, s, :, :, at] = got.reshape(2, NY, 2, 8, width).astype(BF16)
            return carry

        lax.fori_loop(0, D // width, out, 0)

    def bundle(j, lag, i):
        return (i >= lag) & (i < NZ + lag)

    def step(i, carry):
        @pl.when(bundle(i, 0, i))
        def _():
            s = near(z, i)
            for xh in range(2):
                own, _, _ = piece(i, xh)

                @pl.when(jnp.logical_not(own))
                def _(xh=xh):
                    await_bytes(arr.at[c, y, s, xh], a_recv.at[s, xh])

            for copy in own_copies(s):
                copy.start()
            to_partner(y, s).start()

        @pl.when(bundle(i, 1, i))
        def _():
            j = i - 1
            s = near(z, j)
            await_bytes(arr.at[c, down, s], y_recv.at[down, s])

            @pl.when(lax.rem(j, 2) == 0)
            def _():
                onward(down, s, up).start()

            to_partner(down, s).start()
            await_bytes(arr.at[c, up, s], y_recv.at[up, s])

            @pl.when(lax.rem(j, 2) == 1)
            def _():
                onward(up, s, down).start()

            to_partner(up, s).start()

        @pl.when(bundle(i, 2, i))
        def _():
            s = near(z, i - 2)
            await_bytes(arr.at[c, far, s], y_recv.at[far, s])
            to_partner(far, s).start()

        @pl.when(bundle(i, 5, i))
        def _():
            j = i - 5
            s = near(z, j)
            even = lax.rem(j, 2) == 0
            await_bytes(low.at[s], l_recv.at[s])
            to = jnp.where(even, down, up)
            for xh in range(2):
                r1[to, s, xh] = (r1[to, s, xh].astype(F32) + low[s, xh].astype(F32)).astype(BF16)

            @pl.when(even)
            def _():
                joined(s, down, 1).start()

            @pl.when(jnp.logical_not(even))
            def _():
                joined(s, up, 0).start()

        @pl.when(bundle(i, 4, i))
        def _():
            j = i - 4
            s = near(z, j)
            even = lax.rem(j, 2) == 0
            await_bytes(r1.at[:, s], d_recv.at[s])

            def add(n, inner):
                yy = lax.rem(y + 2 + n, NY)
                for xh in range(2):
                    r1[yy, s, xh] = (r1[yy, s, xh].astype(F32) + part[c, yy, s, xh].astype(F32)).astype(BF16)
                return inner

            lax.fori_loop(0, NY, add, 0)

            @pl.when(even)
            def _():
                relay(s, down).start()
                direct(s, up, 0).start()

            @pl.when(jnp.logical_not(even))
            def _():
                relay(s, up).start()
                direct(s, down, 1).start()

        @pl.when(bundle(i, 3, i))
        def _():
            s = near(z, i - 3)

            @pl.when(i == 3)
            def _():
                for copy in loads[4:7]:
                    copy.wait()

            for ysrc in range(NY):
                await_bytes(arr.at[1 - c, ysrc, s], p_recv.at[ysrc, s])
            expert(s)
            over(s).start()

        @pl.when(bundle(i, 6, i))
        def _():
            j = i - 6
            s = near(z, j)
            for side in range(2):
                await_bytes(upd.at[side, s], u_recv.at[side, s])
            for xh in range(2):
                total = r1[y, s, xh].astype(F32) + upd[0, s, xh].astype(F32) + upd[1, s, xh].astype(F32)
                fin[s, xh] = total.astype(BF16)
                own, copy = back(j, xh)

                @pl.when(own)
                def _(xh=xh):
                    ret[s, xh] = fin[s, xh]

                @pl.when(jnp.logical_not(own))
                def _(copy=copy):
                    copy.start()

        pl.when(i == 3)(join_row)
        pl.when(i == 6)(join_planes)
        pl.when(i == 8)(take_state)

        @pl.when(i >= 8)
        def _():
            for k in range(3):
                n = (i - 8) * 3 + k

                @pl.when(n < 16)
                def _(n=n):
                    pass_b_block(n, q_ref, k_ref, v_ref, g_ref, gain_ref, st, mixed)

        return carry

    lax.fori_loop(0, LAST, step, 0)

    def finish(j, carry):
        s = near(z, j)
        for xh in range(2):
            own, sent = exchange(j, xh)
            _, copy = back(j, xh)

            @pl.when(jnp.logical_not(own))
            def _(sent=sent, copy=copy, xh=xh):
                sent.wait_send()
                copy.wait_send()
                await_bytes(ret.at[s, xh], b_recv.at[s, xh])

        for copy in own_copies(s):
            copy.wait_send()
        await_bytes(low.at[s], f_send.at[s])
        for ysrc in range(NY):
            to_partner(ysrc, s).wait_send()
        over(s).wait_send()
        for sem in (l_send, u_send, t_send):
            await_bytes(low.at[s], sem.at[s])
        return carry

    lax.fori_loop(0, NZ, finish, 0)
    for zd in range(1, NZ):

        @pl.when(zd > z)
        def _(zd=zd):
            z_copy(zd).wait_send()

    for d in range(1, NX):
        x1(d).wait_send()
        x2(d).wait_send()

    weights = w_buf[...]
    w_hi = weights.astype(BF16)
    w_low = (weights - w_hi.astype(F32)).astype(BF16)

    def weigh(n, carry):
        at = pl.ds(pl.multiple_of(n * width, width), width)
        got_rows = ret[:, :, :, at].astype(F32).reshape(128, width).astype(BF16)
        got = lax.dot_general(w_hi, got_rows, TN, preferred_element_type=F32)
        got = got + lax.dot_general(w_low, got_rows, TN, preferred_element_type=F32)
        mine[:, at] = jnp.where(c == 0, got[0:32], got[32:64])
        cs[:, at] = jnp.where(c == 0, got[32:64], got[0:32])
        return carry

    lax.fori_loop(0, D // width, weigh, 0)
    swap = remote(cs, cr, c_send, c_recv, c=1 - c)
    swap.start()
    swap.wait()
    total = mine[...] + cr[...]
    scale = lax.rsqrt(jnp.mean(total * total, axis=-1, keepdims=True) + 1e-6)
    routed[...] = (total * scale * post_ref[...]).astype(BF16)


def everything(picks, weights, pre, post, gain, rows, gate, up, down, q, k, v, g):
    dma = pltpu.SemaphoreType.DMA
    vmem = pl.BlockSpec(memory_space=pltpu.VMEM)
    hbm = pl.BlockSpec(memory_space=pl.ANY)
    scratch = [
        pltpu.VMEM((64, D), BF16),
        pltpu.VMEM(gate.shape, BF16),
        pltpu.VMEM(up.shape, BF16),
        pltpu.VMEM(down.shape, BF16),
        pltpu.VMEM(q.shape, BF16),
        pltpu.VMEM(k.shape, BF16),
        pltpu.VMEM(v.shape, BF16),
        pltpu.VMEM(g.shape, F32),
        pltpu.VMEM((16, 8, D), BF16),
        pltpu.VMEM((128, 64), F32),
        pltpu.VMEM((2, NY, NZ, 2, 8, D), BF16),
        pltpu.VMEM((128, D), BF16),
        pltpu.VMEM((2, NY, NZ, 2, 8, D), BF16),
        pltpu.VMEM((NY, NZ, 2, 8, D), BF16),
        pltpu.VMEM((NZ, 2, 8, D), BF16),
        pltpu.VMEM((2, NZ, 2, 8, D), BF16),
        pltpu.VMEM((NZ, 2, 8, D), BF16),
        pltpu.VMEM((NZ, 2, 8, D), BF16),
        pltpu.VMEM((32, D), F32),
        pltpu.VMEM((32, D), F32),
        pltpu.VMEM((32, D), F32),
        pltpu.VMEM((2, DV, DK), F32),
        pltpu.VMEM((1, 2 * DK), F32),
        pltpu.VMEM((4, 2, 80, DK), BF16),
        pltpu.VMEM((4, 2, 80, DK), BF16),
        pltpu.VMEM((2, 80, DK), BF16),
        pltpu.VMEM((NZ, 2, 80, DK), BF16),
        pltpu.VMEM((2, 64, DK), F32),
        pltpu.VMEM((4, 2, 64, DK), F32),
        pltpu.VMEM((4, 2, 64, DK), F32),
        dma((8,)), dma((NZ, 2)), dma((NZ, 2)), dma((2, NZ)), dma((NY, NZ)), dma((NZ,)), dma((NY, NZ)), dma((NY, NZ)),
        dma((3,)), dma((4,)), dma((NZ,)), dma((NZ,)), dma((3,)), dma((4,)),
        dma((NZ,)), dma((NZ,)), dma((NZ,)), dma((NZ,)), dma((NZ,)), dma((NZ,)), dma((2, NZ)),
        dma((NZ, 2)), dma((NZ, 2)), dma(()), dma(()),
    ]
    return pl.pallas_call(
        body,
        out_shape=(
            jax.ShapeDtypeStruct((1024, 2 * DV), BF16),
            jax.ShapeDtypeStruct((32, D), BF16),
        ),
        in_specs=[vmem] * 5 + [hbm] * 8,
        out_specs=[vmem, vmem],
        scratch_shapes=scratch,
        compiler_params=pltpu.CompilerParams(collective_id=0, has_side_effects=True, vmem_limit_bytes=VLIM),
        name="everything",
    )(picks, weights, pre, post, gain, rows, gate, up, down, q, k, v, g)


def on_device(
    queries,
    key_vectors,
    value_vectors,
    decay_logit,
    head_gain,
    routed_rows,
    pre_gain,
    expert_pick,
    route_weight,
    gate_weight,
    up_weight,
    down_weight,
    post_gain,
):
    return everything(
        expert_pick.T,
        route_weight.T,
        pre_gain.reshape(1, D),
        post_gain.reshape(1, D),
        head_gain.reshape(1, DV),
        routed_rows,
        gate_weight[0],
        up_weight[0],
        down_weight[0],
        queries,
        key_vectors,
        value_vectors,
        decay_logit,
    )


def solution(mesh):
    torus = Mesh(mesh.devices.reshape(NZ, NX, NY, 2), ("z", "x", "y", "c"))
    placed = (
        P(EP, TP),
        P(EP, TP),
        P(EP, TP),
        P(EP, TP),
        P(),
        P(EP, None),
        P(),
        P(EP, None),
        P(EP, None),
        P(EP, None, TP),
        P(EP, None, TP),
        P(EP, TP, None),
        P(),
    )
    return jax.shard_map(
        on_device,
        mesh=torus,
        in_specs=placed,
        out_specs=(P(EP, TP), P(EP + TP, None)),
        check_vma=False,
    )
```

time: 161 us -> 119 us (0.74); the launches traced: 158 us -> 117 us
  Pallas kernels: 151 us -> 114 us
  local copies, waits for them, and re-layouts: 5.92 us -> 3.01 us
    pallas_call x4 -> x1, Pallas kernels: 151 us -> 114 us  [everything(): pl.pallas_call(body, out_shape=(jax.ShapeDtypeStruct((1024, 2 * DV), BF16...]
    unnamed x8 -> x4, local copies, waits for them, and re-layouts: 5.1 us -> 3.01 us
where the time goes in v2:
time: 119 us; the launch traced here: 117 us
  Pallas kernels  114 us (96%)
  local copies, waits for them, and re-layouts  3.01 us (3%)
    pallas_call x1, Pallas kernels, everything(): pl.pallas_call(body, out_shape=(jax.ShapeDtypeStruct((1024, 2 * DV), BF16...  114 us
    unnamed x4, local copies, waits for them, and re-layouts  3.01 us

profile of v2, /device:TPU:1, one launch (start us, length us, event | category | flops | bytes accessed | tf_op | source)
XLA Modules:
  0.0 117.4 jit_solution(17275257884293059555)
XLA Ops:
  0.6 113.8 %everything.1 = (bf16[1024,512]{1,0:T(8,128)(2,1)}, bf16[32,4096]{1,0:T(8,128)(2,1)}) custom-call(s32[2,256]{1,0:T(2,128)} %bitcast.13, f32[2,256]{1,0:T(2,128)} %bitcast.14, f32[1,4096]{1,0:T(1,128)} %bitcast.11, f32[1,4096]{1,0:T(1,128)} %bitcast.12, f32[1,256]{1,0:T(1,128)} %bitcast.15, bf16[256,4096]{1,0:T(8,128)(2,1)} %rows_hbm.1, ...), custom_call_target="tpu_custom_call" | custom-call | tf_op jit(solution)/shard_map/everything/pallas_call | solution.py:621
  114.4 0.0 copy-start
  114.4 2.3 %copy.17 = bf16[1024,512]{1,0:T(8,128)(2,1)} copy(bf16[1024,512]{1,0:T(8,128)(2,1)} %get-tuple-element.4) | data formatting | bytes 2097152
  116.7 0.0 copy-done
  116.7 0.7 copy.18
Async XLA Ops:
  114.4 2.3 %copy-start = (bf16[32,4096]{1,0:T(8,128)(2,1)S(1)}, bf16[32,4096]{1,0:T(8,128)(2,1)}, u32[]{:S(2)}) copy-start(bf16[32,4096]{1,0:T(8,128)(2,1)} %get-tuple-element.5) | copy-start | bytes 786436

commit v3 on v2

--- a/solution.py
+++ b/solution.py
@@ -22,7 +22,7 @@
 
 
 def near(z, j):
-    off = jnp.where(lax.rem(j, 2) == 1, (j + 1) // 2, NZ - j // 2)
+    off = jnp.where(j == NZ - 1, 0, jnp.where(lax.rem(j, 2) == 0, j // 2 + 1, NZ - j // 2 - 1))
     return lax.rem(z + off, NZ)
 
 
@@ -566,14 +566,22 @@
         got = lax.dot_general(w_hi, got_rows, TN, preferred_element_type=F32)
         got = got + lax.dot_general(w_low, got_rows, TN, preferred_element_type=F32)
         mine[:, at] = jnp.where(c == 0, got[0:32], got[32:64])
-        cs[:, at] = jnp.where(c == 0, got[32:64], got[0:32])
+        cs[n] = jnp.where(c == 0, got[32:64], got[0:32])
+        swap(n).start()
         return carry
 
+    def swap(n):
+        return remote(cs.at[n], cr.at[n], c_send.at[n], c_recv.at[n], c=1 - c)
+
+    def join(n, carry):
+        at = pl.ds(pl.multiple_of(n * width, width), width)
+        swap(n).wait()
+        mine[:, at] = mine[:, at] + cr[n]
+        return carry
+
     lax.fori_loop(0, D // width, weigh, 0)
-    swap = remote(cs, cr, c_send, c_recv, c=1 - c)
-    swap.start()
-    swap.wait()
-    total = mine[...] + cr[...]
+    lax.fori_loop(0, D // width, join, 0)
+    total = mine[...]
     scale = lax.rsqrt(jnp.mean(total * total, axis=-1, keepdims=True) + 1e-6)
     routed[...] = (total * scale * post_ref[...]).astype(BF16)
 
@@ -602,8 +610,8 @@
         pltpu.VMEM((NZ, 2, 8, D), BF16),
         pltpu.VMEM((NZ, 2, 8, D), BF16),
         pltpu.VMEM((32, D), F32),
-        pltpu.VMEM((32, D), F32),
-        pltpu.VMEM((32, D), F32),
+        pltpu.VMEM((8, 32, D // 8), F32),
+        pltpu.VMEM((8, 32, D // 8), F32),
         pltpu.VMEM((2, DV, DK), F32),
         pltpu.VMEM((1, 2 * DK), F32),
         pltpu.VMEM((4, 2, 80, DK), BF16),
@@ -616,7 +624,7 @@
         dma((8,)), dma((NZ, 2)), dma((NZ, 2)), dma((2, NZ)), dma((NY, NZ)), dma((NZ,)), dma((NY, NZ)), dma((NY, NZ)),
         dma((3,)), dma((4,)), dma((NZ,)), dma((NZ,)), dma((3,)), dma((4,)),
         dma((NZ,)), dma((NZ,)), dma((NZ,)), dma((NZ,)), dma((NZ,)), dma((NZ,)), dma((2, NZ)),
-        dma((NZ, 2)), dma((NZ, 2)), dma(()), dma(()),
+        dma((NZ, 2)), dma((NZ, 2)), dma((8,)), dma((8,)),
     ]
     return pl.pallas_call(
         body,

time: 119 us -> 113 us (0.950); the launches traced: 117 us -> 113 us
  Pallas kernels: 114 us -> 109 us
    pallas_call x1, Pallas kernels: 114 us -> 109 us  [everything(): pl.pallas_call(body, out_shape=(jax.ShapeDtypeStruct((1024, 2 * DV), BF16...]
where the time goes in v3:
time: 113 us
  Pallas kernels  109 us (96%)
  local copies, waits for them, and re-layouts  3.01 us (3%)
    pallas_call x1, Pallas kernels, everything(): pl.pallas_call(body, out_shape=(jax.ShapeDtypeStruct((1024, 2 * DV), BF16...  109 us
    unnamed x4, local copies, waits for them, and re-layouts  3.01 us

profile of v3, /device:TPU:1, one launch (start us, length us, event | category | flops | bytes accessed | tf_op | source)
XLA Modules:
  0.0 113.0 jit_solution(2424046556921801845)
XLA Ops:
  0.6 109.4 %everything.1 = (bf16[1024,512]{1,0:T(8,128)(2,1)}, bf16[32,4096]{1,0:T(8,128)(2,1)}) custom-call(s32[2,256]{1,0:T(2,128)} %bitcast.13, f32[2,256]{1,0:T(2,128)} %bitcast.14, f32[1,4096]{1,0:T(1,128)} %bitcast.11, f32[1,4096]{1,0:T(1,128)} %bitcast.12, f32[1,256]{1,0:T(1,128)} %bitcast.15, bf16[256,4096]{1,0:T(8,128)(2,1)} %rows_hbm.1, ...), custom_call_target="tpu_custom_call" | custom-call | tf_op jit(solution)/shard_map/everything/pallas_call | solution.py:629
  110.0 0.0 copy-start
  110.0 2.3 %copy.17 = bf16[1024,512]{1,0:T(8,128)(2,1)} copy(bf16[1024,512]{1,0:T(8,128)(2,1)} %get-tuple-element.4) | data formatting | bytes 2097152
  112.3 0.0 copy-done
  112.3 0.7 copy.18
Async XLA Ops:
  110.0 2.3 %copy-start = (bf16[32,4096]{1,0:T(8,128)(2,1)S(1)}, bf16[32,4096]{1,0:T(8,128)(2,1)}, u32[]{:S(2)}) copy-start(bf16[32,4096]{1,0:T(8,128)(2,1)} %get-tuple-element.5) | copy-start | bytes 786436

commit v4 on v3

--- a/solution.py
+++ b/solution.py
@@ -158,7 +158,7 @@
         st_ref[h] = state * decay[:, ks] + update
 
 
-LAST = NZ + 6
+LAST = NZ + 5
 
 
 def body(
@@ -430,9 +430,9 @@
             await_bytes(arr.at[c, far, s], y_recv.at[far, s])
             to_partner(far, s).start()
 
-        @pl.when(bundle(i, 5, i))
-        def _():
-            j = i - 5
+        @pl.when(bundle(i, 4, i))
+        def _():
+            j = i - 4
             s = near(z, j)
             even = lax.rem(j, 2) == 0
             await_bytes(low.at[s], l_recv.at[s])
@@ -448,9 +448,9 @@
             def _():
                 joined(s, up, 0).start()
 
-        @pl.when(bundle(i, 4, i))
-        def _():
-            j = i - 4
+        @pl.when(bundle(i, 3, i))
+        def _():
+            j = i - 3
             s = near(z, j)
             even = lax.rem(j, 2) == 0
             await_bytes(r1.at[:, s], d_recv.at[s])
@@ -473,11 +473,11 @@
                 relay(s, up).start()
                 direct(s, down, 1).start()
 
-        @pl.when(bundle(i, 3, i))
-        def _():
-            s = near(z, i - 3)
-
-            @pl.when(i == 3)
+        @pl.when(bundle(i, 2, i))
+        def _():
+            s = near(z, i - 2)
+
+            @pl.when(i == 2)
             def _():
                 for copy in loads[4:7]:
                     copy.wait()
@@ -487,9 +487,9 @@
             expert(s)
             over(s).start()
 
-        @pl.when(bundle(i, 6, i))
-        def _():
-            j = i - 6
+        @pl.when(bundle(i, 5, i))
+        def _():
+            j = i - 5
             s = near(z, j)
             for side in range(2):
                 await_bytes(upd.at[side, s], u_recv.at[side, s])
@@ -508,12 +508,12 @@
 
         pl.when(i == 3)(join_row)
         pl.when(i == 6)(join_planes)
-        pl.when(i == 8)(take_state)
-
-        @pl.when(i >= 8)
+        pl.when(i == 7)(take_state)
+
+        @pl.when(i >= 7)
         def _():
             for k in range(3):
-                n = (i - 8) * 3 + k
+                n = (i - 7) * 3 + k
 
                 @pl.when(n < 16)
                 def _(n=n):

time: 113 us -> 114 us (level)
  no operation moved by 1% of the time
where the time goes in v4:
time: 114 us; the launch traced here: 113 us
  Pallas kernels  110 us (96%)
  local copies, waits for them, and re-layouts  3.01 us (3%)
    pallas_call x1, Pallas kernels, everything(): pl.pallas_call(body, out_shape=(jax.ShapeDtypeStruct((1024, 2 * DV), BF16...  110 us
    unnamed x4, local copies, waits for them, and re-layouts  3.01 us

profile of v4, /device:TPU:1, one launch (start us, length us, event | category | flops | bytes accessed | tf_op | source)
XLA Modules:
  0.0 113.4 jit_solution(14404307020991062117)
XLA Ops:
  0.6 109.7 %everything.1 = (bf16[1024,512]{1,0:T(8,128)(2,1)}, bf16[32,4096]{1,0:T(8,128)(2,1)}) custom-call(s32[2,256]{1,0:T(2,128)} %bitcast.13, f32[2,256]{1,0:T(2,128)} %bitcast.14, f32[1,4096]{1,0:T(1,128)} %bitcast.11, f32[1,4096]{1,0:T(1,128)} %bitcast.12, f32[1,256]{1,0:T(1,128)} %bitcast.15, bf16[256,4096]{1,0:T(8,128)(2,1)} %rows_hbm.1, ...), custom_call_target="tpu_custom_call" | custom-call | tf_op jit(solution)/shard_map/everything/pallas_call | solution.py:629
  110.4 0.0 copy-start
  110.4 2.3 %copy.17 = bf16[1024,512]{1,0:T(8,128)(2,1)} copy(bf16[1024,512]{1,0:T(8,128)(2,1)} %get-tuple-element.4) | data formatting | bytes 2097152
  112.7 0.0 copy-done
  112.7 0.7 copy.18
Async XLA Ops:
  110.4 2.3 %copy-start = (bf16[32,4096]{1,0:T(8,128)(2,1)S(1)}, bf16[32,4096]{1,0:T(8,128)(2,1)}, u32[]{:S(2)}) copy-start(bf16[32,4096]{1,0:T(8,128)(2,1)} %get-tuple-element.5) | copy-start | bytes 786436
